TPU v7x, 512 devices: a whole 4x4x16 slice. The times are simulated.
512 devices in a mesh: ep: 32 (over z, core), tp: 16 (over y, x).
Axes of the slice: x: 4, y: 4, z: 16, core: 2. Of those that a mesh axis runs over, the one named last changes fastest.
Arguments:
- query_maps: bfloat16 [8192, 4096], P('ep', 'tp'), may hold values from -40 to 40
- key_maps: bfloat16 [8192, 4096], P('ep', 'tp'), may hold values from -40 to 40
- value_rows: bfloat16 [8192, 4096], P('ep', 'tp'), may hold values from -6 to 6
- head_lambda: float32 [16], P('tp'), may hold values from 0.3 to 0.8
- head_gain: float32 [256], replicated, may hold values from 0.1 to 1.9
- out_weight: bfloat16 [4096, 2048], P('tp'), may hold values from -0.125 to 0.125
- expert_rows: bfloat16 [4096, 2048], P('ep'), may hold values from -6 to 6
- expert_gain: float32 [2048], replicated, may hold values from 0.1 to 1.9
- routes: int32 [4096, 2], P('ep'), may hold values from 0 to 31, all different within a row; in each aligned block of 128 rows (0 to 127, 128 to 255, ...) at most 12 rows name the same one
- route_weights: float32 [4096, 2], P('ep'), may hold values from 0.2 to 1
- gate_weight: bfloat16 [32, 2048, 4096], P('ep', None, 'tp'), may hold values from -0.125 to 0.125
- up_weight: bfloat16 [32, 2048, 4096], P('ep', None, 'tp'), may hold values from -0.125 to 0.125
- down_weight: bfloat16 [32, 4096, 2048], P('ep', 'tp'), may hold values from -0.125 to 0.125
Outputs:
- mixed: bfloat16 [8192, 2048], P('ep', 'tp')
- expert_out: bfloat16 [4096, 2048], P('ep', 'tp')
Inputs may be any that keep to these rules, and one draw needn't show every extreme that they name: `routes`: within the rows of one device (aligned blocks of 128 rows) no expert is named more than 12 times, and the 2 experts of a row differ.
All inputs are finite; a program needn't handle non-finite values.
Results may differ from a plain program's by a relative error of at most 0.018.
Values may be sent and summed in bfloat16 or wider, within the bound.
No kernel may reach another device: no remote copies, remote signals or barrier semaphores. Data moves between devices by JAX's collectives and lax.ppermute only.
A program may use at most 128 MiB of HBM per device.

v0:
```python
import functools

import jax
import jax.numpy as jnp
from jax import lax
from jax.experimental import pallas as pl
from jax.experimental.pallas import tpu as pltpu
from jax.sharding import PartitionSpec as P


norm_eps = 1e-06
rope_base = 10000.0
low = -1e30
log2e = 1.4426950408889634


def vmem(count):
    return [pl.BlockSpec(memory_space=pltpu.VMEM) for _ in range(count)]


def near(x):
    return pltpu.with_memory_space_constraint(x, pltpu.VMEM)


def far(x):
    return pltpu.with_memory_space_constraint(x, pltpu.HBM)


def hbm(count):
    return [pl.BlockSpec(memory_space=pltpu.HBM) for _ in range(count)]


def start_copies(sources, targets, semaphores):
    copies = [
        pltpu.make_async_copy(a, b, semaphores.at[i])
        for i, (a, b) in enumerate(zip(sources, targets))
    ]
    for copy in copies:
        copy.start()
    return copies


def smem(count):
    return [pl.BlockSpec(memory_space=pltpu.SMEM) for _ in range(count)]


def dot_f32(a, b, dims):
    return lax.dot_general(a, b, (dims, ((), ())), preferred_element_type=jnp.float32)


def turn_kernel(q_hbm, k_hbm, v_hbm, cos_ref, sin_ref, q_out, kv_out, q_ref, k_ref, semaphores):
    copies = start_copies(
        (q_hbm, k_hbm, v_hbm), (q_ref, k_ref, kv_out.at[:, pl.ds(256, 256)]), semaphores
    )
    cos_table = cos_ref[...]
    sin_table = sin_ref[...]

    def turned(x):
        x = x.astype(jnp.float32)
        return (x * cos_table + pltpu.roll(x, 64, 1) * sin_table).astype(jnp.bfloat16)

    for ref, out, copy in ((q_ref, q_out, copies[0]), (k_ref, kv_out, copies[1])):
        copy.wait()
        for m in range(2):
            at = slice(128 * m, 128 * (m + 1))
            out[:, at] = turned(ref[:, at])
    copies[2].wait()


def turn(q, k, v, offset):
    rows = q.shape[0]
    lane = jnp.arange(128, dtype=jnp.int32)
    inverse = rope_base ** (-2.0 * (lane % 64).astype(jnp.float32) / 128)
    positions = (offset + jnp.arange(rows, dtype=jnp.int32)).astype(jnp.float32)
    angles = positions[:, None] * inverse[None, :]
    cos_table = jnp.cos(angles)
    sin_table = jnp.sin(angles) * jnp.where(lane < 64, -1.0, 1.0)[None, :]
    return pl.pallas_call(
        turn_kernel,
        out_shape=(
            pltpu.VMEM((rows, 256), jnp.bfloat16),
            pltpu.VMEM((rows, 512), jnp.bfloat16),
        ),
        compiler_params=pltpu.CompilerParams(vmem_limit_bytes=24 * 2**20),
        in_specs=hbm(3) + vmem(2),
        out_specs=tuple(vmem(2)),
        scratch_shapes=[
            pltpu.VMEM((rows, 256), jnp.bfloat16),
            pltpu.VMEM((rows, 256), jnp.bfloat16),
            pltpu.SemaphoreType.DMA((3,)),
        ],
        name="turn",
    )(far(q), far(k), far(v), near(cos_table), near(sin_table))


chunk = 1024


def attend_kernel(ep_ref, lam_ref, *refs):
    sources, refs = refs[:4], refs[4:]
    kv_hbm = sources[3]
    out_ref, q_ref, weight_ref, gain_ref, kv_buf, top_ref, mass_ref, acc_ref = refs[:8]
    semaphores, kv_semaphores = refs[8:]
    ep = ep_ref[0]
    full = ep * 256 // chunk
    factor = (128.0**-0.5) * log2e
    copies = start_copies((sources[0],), (q_ref,), semaphores)

    def chunk_copy(j):
        at = pl.ds(pl.multiple_of(j * chunk, chunk), chunk)
        return pltpu.make_async_copy(kv_hbm.at[at, :], kv_buf.at[j], kv_semaphores.at[j])

    lax.fori_loop(0, full + 1, lambda j, c: (chunk_copy(j).start(), c)[1], 0)
    late = start_copies(
        sources[1:3], (weight_ref, gain_ref), semaphores.at[pl.ds(1, 2)]
    )
    top_ref[...] = jnp.full(top_ref.shape, low, jnp.float32)
    mass_ref[...] = jnp.zeros(mass_ref.shape, jnp.float32)
    acc_ref[...] = jnp.zeros(acc_ref.shape, jnp.float32)
    copies[0].wait()

    def fold(j, masked):
        for m in range(2):
            q = q_ref[:, 128 * m : 128 * (m + 1)]
            s = dot_f32(q, kv_buf[j, :, 128 * m : 128 * (m + 1)], ((1,), (1,)))
            if masked:
                row = ep * 256 + lax.broadcasted_iota(jnp.int32, (256, chunk), 0)
                col = j * chunk + lax.broadcasted_iota(jnp.int32, (256, chunk), 1)
                s = jnp.where(col <= row, s, low)
            pieces = [s[:, 128 * i : 128 * (i + 1)] for i in range(chunk // 128)]
            peak = jnp.max(functools.reduce(jnp.maximum, pieces), axis=1, keepdims=True)
            before = top_ref[m, :, 0:1]
            peak = jnp.maximum(peak * factor, before)
            rescale = jnp.exp2(before - peak)
            top_ref[m] = jnp.broadcast_to(peak, (256, 128))
            p = jnp.exp2(s * factor - peak)
            pieces = [p[:, 128 * i : 128 * (i + 1)] for i in range(chunk // 128)]
            mass_ref[m] = mass_ref[m] * rescale + functools.reduce(jnp.add, pieces)
            gained = dot_f32(p.astype(jnp.bfloat16), kv_buf[j, :, 256:], ((1,), (0,)))
            acc_ref[m] = acc_ref[m] * rescale + gained

    def step(j, c):
        chunk_copy(j).wait()
        fold(j, False)
        return c

    lax.fori_loop(0, full, step, 0)
    chunk_copy(full).wait()
    fold(full, True)
    maps = [acc_ref[m] / jnp.sum(mass_ref[m], axis=1, keepdims=True) for m in range(2)]
    difference = maps[0] - lam_ref[0] * maps[1]
    mean = jnp.mean(difference * difference, axis=1, keepdims=True)
    for copy in late:
        copy.wait()
    head = (difference * lax.rsqrt(mean + norm_eps) * gain_ref[...]).astype(jnp.bfloat16)
    for j in range(8):
        part = dot_f32(head, weight_ref[:, 256 * j : 256 * (j + 1)], ((1,), (0,)))
        part = part.astype(jnp.bfloat16)
        out_ref[2 * j] = part[:, :128]
        out_ref[2 * j + 1] = part[:, 128:]


def attend(ep, lam, q, kv, gain, weight):
    return pl.pallas_call(
        attend_kernel,
        out_shape=pltpu.VMEM((16, 256, 128), jnp.bfloat16),
        compiler_params=pltpu.CompilerParams(vmem_limit_bytes=40 * 2**20),
        in_specs=smem(2) + hbm(4),
        out_specs=vmem(1)[0],
        scratch_shapes=[
            pltpu.VMEM((256, 256), jnp.bfloat16),
            pltpu.VMEM(weight.shape, jnp.bfloat16),
            pltpu.VMEM((1, 256), jnp.float32),
            pltpu.VMEM((kv.shape[0] // chunk, chunk, 512), jnp.bfloat16),
            pltpu.VMEM((2, 256, 128), jnp.float32),
            pltpu.VMEM((2, 256, 128), jnp.float32),
            pltpu.VMEM((2, 256, 256), jnp.float32),
            pltpu.SemaphoreType.DMA((3,)),
            pltpu.SemaphoreType.DMA((kv.shape[0] // chunk,)),
        ],
        cost_estimate=pl.CostEstimate(
            flops=2 * 256 * kv.shape[0] * 2 * 512,
            transcendentals=256 * kv.shape[0] * 2,
            bytes_accessed=kv.shape[0] * 1024,
        ),
        name="attend",
    )(ep, lam, far(q), far(weight), far(gain.reshape(1, 256)), far(kv))


def slots_of(routes_ref):
    expert = lax.broadcasted_iota(jnp.int32, (32, 128), 0)
    first = routes_ref[0:1, :] == expert
    second = routes_ref[1:2, :] == expert
    named = jnp.where(first | second, 1.0, 0.0).astype(jnp.bfloat16)
    before = lax.broadcasted_iota(jnp.int32, (128, 128), 0)
    after = lax.broadcasted_iota(jnp.int32, (128, 128), 1)
    earlier = jnp.where(before < after, 1.0, 0.0).astype(jnp.bfloat16)
    slot = dot_f32(named, earlier, ((1,), (0,))).astype(jnp.int32)
    return first, second, slot


def chosen(named, slot):
    where = jnp.where(named, slot, -1)[:, None, :]
    index = lax.broadcasted_iota(jnp.int32, (32, 16, 128), 1)
    return jnp.where(where == index, 1.0, 0.0).reshape(512, 128).astype(jnp.bfloat16)


def pack_kernel(tp_ref, *refs):
    sources, (out_ref, rows_ref, gain_ref, routes_ref, semaphores) = refs[:3], refs[3:]
    copies = start_copies(sources, (rows_ref, gain_ref, routes_ref), semaphores)
    copies[2].wait()
    first, second, slot = slots_of(routes_ref)
    pick = chosen(first | second, slot)
    copies[0].wait()
    copies[1].wait()
    x = rows_ref[...].astype(jnp.float32)
    inverse = lax.rsqrt(jnp.mean(x * x, axis=1, keepdims=True) + norm_eps)
    start = pl.multiple_of(tp_ref[0] * 128, 128)
    mine = rows_ref[:, pl.ds(start, 128)].astype(jnp.float32)
    normed = (mine * inverse * gain_ref[:, pl.ds(start, 128)]).astype(jnp.bfloat16)
    packed = dot_f32(pick, normed, ((1,), (0,)))
    out_ref[...] = packed.astype(jnp.bfloat16).reshape(32, 16, 128)


def pack(tp, rows, gain, routes_t):
    return pl.pallas_call(
        pack_kernel,
        out_shape=pltpu.VMEM((32, 16, 128), jnp.bfloat16),
        compiler_params=pltpu.CompilerParams(vmem_limit_bytes=24 * 2**20),
        in_specs=smem(1) + hbm(3),
        out_specs=vmem(1)[0],
        scratch_shapes=[
            pltpu.VMEM(rows.shape, jnp.bfloat16),
            pltpu.VMEM((1, rows.shape[1]), jnp.float32),
            pltpu.VMEM(routes_t.shape, jnp.int32),
            pltpu.SemaphoreType.DMA((3,)),
        ],
        name="pack",
    )(tp, far(rows), far(gain.reshape(1, -1)), far(routes_t))


def dense_slots(shape, slot_dim):
    slot = lax.broadcasted_iota(jnp.int32, shape, slot_dim)
    row = lax.broadcasted_iota(jnp.int32, shape, 1 - slot_dim)
    place = jnp.where((slot & 15) < 12, (slot >> 4) * 12 + (slot & 15), -1)
    return jnp.where(place == row, 1.0, 0.0).astype(jnp.bfloat16)


def squeeze_kernel(arrived_ref, out_ref):
    slots = arrived_ref[...].reshape(512, 128)
    rows = dot_f32(dense_slots((384, 512), 1), slots, ((1,), (0,))).astype(jnp.bfloat16)
    for j in range(16):
        out_ref[j] = rows


def squeeze(arrived):
    return pl.pallas_call(
        squeeze_kernel,
        out_shape=pltpu.VMEM((16, 384, 128), jnp.bfloat16),
        compiler_params=pltpu.CompilerParams(vmem_limit_bytes=24 * 2**20),
        in_specs=vmem(1),
        out_specs=vmem(1)[0],
        name="squeeze",
    )(near(arrived))


def ffn_kernel(rows_ref, *refs):
    sources, (out_ref, gate_ref, up_ref, down_ref, semaphores) = refs[:3], refs[3:]
    copies = start_copies(sources, (gate_ref, up_ref, down_ref), semaphores)
    gate = jnp.zeros((384, 256), jnp.float32)
    up = jnp.zeros((384, 256), jnp.float32)
    copies[0].wait()
    for j in range(8):
        x = jnp.concatenate([rows_ref[2 * j], rows_ref[2 * j + 1]], axis=1)
        gate = gate + dot_f32(x, gate_ref[256 * j : 256 * (j + 1), :], ((1,), (0,)))
    copies[1].wait()
    for j in range(8):
        x = jnp.concatenate([rows_ref[2 * j], rows_ref[2 * j + 1]], axis=1)
        up = up + dot_f32(x, up_ref[256 * j : 256 * (j + 1), :], ((1,), (0,)))
    copies[2].wait()
    hidden = (gate / (1.0 + jnp.exp(-gate)) * up).astype(jnp.bfloat16)
    for j in range(8):
        part = dot_f32(hidden, down_ref[:, 256 * j : 256 * (j + 1)], ((1,), (0,)))
        part = part.astype(jnp.bfloat16)
        out_ref[2 * j] = part[:, :128]
        out_ref[2 * j + 1] = part[:, 128:]


def ffn(rows, gate, up, down):
    return pl.pallas_call(
        ffn_kernel,
        out_shape=pltpu.VMEM((16, 384, 128), jnp.bfloat16),
        compiler_params=pltpu.CompilerParams(vmem_limit_bytes=24 * 2**20),
        in_specs=vmem(1) + hbm(3),
        out_specs=vmem(1)[0],
        scratch_shapes=[
            pltpu.VMEM(gate.shape, jnp.bfloat16),
            pltpu.VMEM(up.shape, jnp.bfloat16),
            pltpu.VMEM(down.shape, jnp.bfloat16),
            pltpu.SemaphoreType.DMA((3,)),
        ],
        cost_estimate=pl.CostEstimate(
            flops=2 * 384 * 2048 * 768, transcendentals=384 * 256, bytes_accessed=6 * 2**20
        ),
        name="ffn",
    )(near(rows), far(gate), far(up), far(down))


def total_kernel(parts_ref, out_ref):
    total = parts_ref[0].astype(jnp.float32)
    for j in range(1, 16):
        total = total + parts_ref[j].astype(jnp.float32)
    rows = total.astype(jnp.bfloat16)
    slots = dot_f32(dense_slots((512, 384), 0), rows, ((1,), (0,)))
    out_ref[...] = slots.astype(jnp.bfloat16).reshape(32, 16, 128)


def total_of(parts):
    return pl.pallas_call(
        total_kernel,
        out_shape=pltpu.VMEM((32, 16, 128), jnp.bfloat16),
        compiler_params=pltpu.CompilerParams(vmem_limit_bytes=24 * 2**20),
        in_specs=vmem(1),
        out_specs=vmem(1)[0],
        name="total",
    )(near(parts))


def combine_kernel(returned_ref, routes_ref, weights_ref, out_ref):
    slots = returned_ref[...].reshape(512, 128)
    first, second, slot = slots_of(routes_ref)
    one = dot_f32(chosen(first, slot), slots, ((0,), (0,)))
    two = dot_f32(chosen(second, slot), slots, ((0,), (0,)))
    out = weights_ref[:, 0:1] * one + weights_ref[:, 1:2] * two
    out_ref[...] = out.astype(jnp.bfloat16)


def combine(returned, routes_t, weights):
    return pl.pallas_call(
        combine_kernel,
        out_shape=jax.ShapeDtypeStruct((128, 128), jnp.bfloat16),
        compiler_params=pltpu.CompilerParams(vmem_limit_bytes=24 * 2**20),
        in_specs=vmem(3),
        out_specs=vmem(1)[0],
        name="combine",
    )(near(returned), routes_t, weights)


def exchange(blocks, axis):
    return lax.all_to_all(blocks, axis, split_axis=0, concat_axis=0, tiled=True)


def on_device(
    query_maps,
    key_maps,
    value_rows,
    head_lambda,
    head_gain,
    out_weight,
    expert_rows,
    expert_gain,
    routes,
    route_weights,
    gate_weight,
    up_weight,
    down_weight,
):
    return step_of(
        query_maps,
        key_maps,
        value_rows,
        head_lambda,
        head_gain,
        out_weight,
        expert_rows,
        expert_gain,
        routes,
        route_weights,
        gate_weight[0],
        up_weight[0],
        down_weight[0],
    )


def step_of(
    query_maps,
    key_maps,
    value_rows,
    head_lambda,
    head_gain,
    out_weight,
    expert_rows,
    expert_gain,
    routes,
    route_weights,
    gate_weight,
    up_weight,
    down_weight,
):
    ep = lax.axis_index("ep")
    tp = lax.axis_index("tp")
    routes_t = routes.T
    packed = pack(tp.reshape(1), expert_rows, expert_gain, routes_t)
    arrived = exchange(packed, "ep")
    own_q, own_kv = turn(query_maps, key_maps, value_rows, ep * query_maps.shape[0])
    kv = lax.all_gather(own_kv, "ep", axis=0, tiled=True)
    gathered = exchange(squeeze(arrived), "tp")
    parts = ffn(gathered, gate_weight, up_weight, down_weight)
    summed = total_of(exchange(parts, "tp"))
    returned = exchange(summed, "ep")

    partial_value = attend(ep.reshape(1), head_lambda, own_q, kv, head_gain, out_weight)
    mixed_parts = exchange(partial_value, "tp")
    mixed = mixed_parts.astype(jnp.float32).sum(axis=0).astype(jnp.bfloat16)
    expert_out = combine(returned, routes_t, route_weights)
    return (mixed, expert_out)


def solution(mesh):
    placed = (
        P("ep", "tp"),
        P("ep", "tp"),
        P("ep", "tp"),
        P("tp"),
        P(),
        P("tp", None),
        P("ep", None),
        P(),
        P("ep", None),
        P("ep", None),
        P("ep", None, "tp"),
        P("ep", None, "tp"),
        P("ep", "tp", None),
    )
    return jax.shard_map(
        on_device,
        mesh=mesh,
        in_specs=placed,
        out_specs=(P("ep", "tp"), P("ep", "tp")),
        check_vma=False,
    )
```

profile of v0, /device:TPU:64, one launch (start us, length us, event | category | flops | bytes accessed | tf_op | source)
XLA Modules:
  0.0 152.8 jit_solution(16235481304345488781)
XLA Ops:
  7.2 0.0 all-gather.2.cloned.1.call-start
  7.2 0.5 fusion
  7.8 1.9 %turn.1 = (bf16[256,256]{1,0:T(8,128)(2,1)S(1)}, bf16[256,512]{1,0:T(8,128)(2,1)}) custom-call(bf16[256,256]{1,0:T(8,128)(2,1)} %q_hbm.1, bf16[256,256]{1,0:T(8,128)(2,1)} %k_hbm.1, bf16[256,256]{1,0:T(8,128)(2,1)} %v_hbm.1, f32[256,128]{1,0:T(8,128)S(1)} %get-tuple-element.7.cos_ref, f32[256,128]{1,0:T(8,128)S(1)} %get-tuple-element.6.sin_ref), custom_call_target="tpu_custom_call" | custom-call | tf_op jit(solution)/shard_map/turn/pallas_call | solution.py:78
  9.7 0.0 copy-start.1
  9.7 0.6 copy-done.1
  10.3 0.0 all-gather.2.cloned.1.call-update
  10.4 1.4 pack.1
  11.8 29.1 %all_to_all.25.arrived_ref = bf16[32,16,128]{2,1,0:T(8,128)(2,1)S(1)} all-to-all(bf16[32,16,128]{2,1,0:T(8,128)(2,1)S(1)} %pack.1), channel_id=1, replica_groups=mesh['ep'=32,'tp'=16] {'ep'}, dimensions={0} | all-to-all | bytes 262144 | tf_op jit(solution)/shard_map/all_to_all | solution.py:350
  40.9 0.3 squeeze.13
  41.2 31.2 %all_to_all.26.rows_ref = bf16[16,384,128]{2,1,0:T(8,128)(2,1)S(1)} all-to-all(bf16[16,384,128]{2,1,0:T(8,128)(2,1)S(1)} %squeeze.13), channel_id=1, replica_groups=mesh['ep'=32,'tp'=16] {'tp'}, dimensions={0} | all-to-all | bytes 3145728 | tf_op jit(solution)/shard_map/all_to_all | solution.py:350
  72.5 3.8 %ffn.1 = bf16[16,384,128]{2,1,0:T(8,128)(2,1)S(1)} custom-call(bf16[16,384,128]{2,1,0:T(8,128)(2,1)S(1)} %all_to_all.26.rows_ref, bf16[2048,256]{1,0:T(8,128)(2,1)} %bitcast.10, bf16[2048,256]{1,0:T(8,128)(2,1)} %bitcast.11, bf16[256,2048]{1,0:T(8,128)(2,1)} %bitcast.12), custom_call_target="tpu_custom_call" | custom-call | flops 1207959552 | bytes 6291456 | tf_op jit(solution)/shard_map/ffn/pallas_call | solution.py:290
  76.2 25.7 %all_to_all.27.parts_ref = bf16[16,384,128]{2,1,0:T(8,128)(2,1)S(1)} all-to-all(bf16[16,384,128]{2,1,0:T(8,128)(2,1)S(1)} %ffn.1), channel_id=1, replica_groups=mesh['ep'=32,'tp'=16] {'tp'}, dimensions={0} | all-to-all | bytes 3145728 | tf_op jit(solution)/shard_map/all_to_all | solution.py:350
  102.0 1.1 total.1
  103.1 5.0 %all-to-all-start.4 = ((bf16[32,16,128]{2,1,0:T(8,128)(2,1)}), bf16[32,16,128]{2,1,0:T(8,128)(2,1)S(1)}, u32[]{:S(2)}, u32[]{:S(2)}) async-start(bf16[32,16,128]{2,1,0:T(8,128)(2,1)} %total.1), calls=%async_computation.4 | async-start | bytes 262144 | tf_op jit(solution)/shard_map/all_to_all | solution.py:350
  108.8 0.0 all-gather.2.cloned.1.call-done.refs_3_
  108.8 5.8 %attend.1 = bf16[16,256,128]{2,1,0:T(8,128)(2,1)} custom-call(s32[1]{0:T(128)} %bitcast.ep_ref, f32[1]{0:T(128)S(6)} %copy.16.lam_ref, bf16[256,256]{1,0:T(8,128)(2,1)} %copy-done.1, bf16[256,2048]{1,0:T(8,128)(2,1)} %refs_1_.1, f32[1,256]{1,0:T(1,128)} %bitcast.14, bf16[8192,512]{1,0:T(8,128)(2,1)} %all-gather.2.cloned.1.call-done.refs_3_), custom_call_target="tpu_custom_call" | custom-call | flops 4294967296 | bytes 8388608 | tf_op jit(solution)/shard_map/attend/pallas_call | solution.py:164
  114.6 0.0 copy-start.2
  114.6 0.0 copy-start
  114.6 7.7 %all-to-all-done.4.returned_ref = bf16[32,16,128]{2,1,0:T(8,128)(2,1)S(1)} async-done(((bf16[32,16,128]{2,1,0:T(8,128)(2,1)}), bf16[32,16,128]{2,1,0:T(8,128)(2,1)S(1)}, u32[]{:S(2)}, u32[]{:S(2)}) %all-to-all-start.4) | async-done | bytes 131104 | tf_op jit(solution)/shard_map/all_to_all | solution.py:350
  122.3 3.7 %all-to-all-start = ((bf16[16,256,128]{2,1,0:T(8,128)(2,1)}), bf16[16,256,128]{2,1,0:T(8,128)(2,1)S(1)}, u32[]{:S(2)}, u32[]{:S(2)}) async-start(bf16[16,256,128]{2,1,0:T(8,128)(2,1)} %attend.1), calls=%async_computation | async-start | bytes 2097152 | tf_op jit(solution)/shard_map/all_to_all | solution.py:350
  126.0 0.0 copy-done.2
  126.0 0.1 copy.15.weights_ref
  126.1 0.0 copy-done
  126.1 1.0 combine.1
  127.1 18.1 %all-to-all-done = bf16[16,256,128]{2,1,0:T(8,128)(2,1)S(1)} async-done(((bf16[16,256,128]{2,1,0:T(8,128)(2,1)}), bf16[16,256,128]{2,1,0:T(8,128)(2,1)S(1)}, u32[]{:S(2)}, u32[]{:S(2)}) %all-to-all-start) | async-done | bytes 1048608 | tf_op jit(solution)/shard_map/all_to_all | solution.py:350
  145.2 0.8 reduce_sum.12
  (2 shorter events, 0.0 us)
Async XLA Ops:
  7.2 101.6 %all-gather.2.cloned.1.call-start = ((), (), s32[]{:S(2)}) async-start(), calls=%async_computation.5 | async-start | bytes 8650752 | tf_op jit(solution)/shard_map/all_gather | solution.py:406
  9.7 0.6 copy-start.1
  103.1 19.2 %all-to-all-start.4 = ((bf16[32,16,128]{2,1,0:T(8,128)(2,1)}), bf16[32,16,128]{2,1,0:T(8,128)(2,1)S(1)}, u32[]{:S(2)}, u32[]{:S(2)}) async-start(bf16[32,16,128]{2,1,0:T(8,128)(2,1)} %total.1), calls=%async_computation.4 | async-start | bytes 262144 | tf_op jit(solution)/shard_map/all_to_all | solution.py:350
  114.6 11.4 %copy-start.2 = (f32[128,2]{0,1:T(2,128)S(1)}, f32[128,2]{0,1:T(2,128)}, u32[]{:S(2)}) copy-start(f32[128,2]{0,1:T(2,128)} %param.22) | copy-start | bytes 3076
  114.6 11.5 %copy-start = (s32[128,2]{0,1:T(2,128)S(1)}, s32[128,2]{0,1:T(2,128)}, u32[]{:S(2)}) copy-start(s32[128,2]{0,1:T(2,128)} %param.21) | copy-start | bytes 3076
  122.3 22.9 %all-to-all-start = ((bf16[16,256,128]{2,1,0:T(8,128)(2,1)}), bf16[16,256,128]{2,1,0:T(8,128)(2,1)S(1)}, u32[]{:S(2)}, u32[]{:S(2)}) async-start(bf16[16,256,128]{2,1,0:T(8,128)(2,1)} %attend.1), calls=%async_computation | async-start | bytes 2097152 | tf_op jit(solution)/shard_map/all_to_all | solution.py:350
Sparse Core Ops, SparseCore 0:
  10.5 83.1 all-gather.1
where the time goes:
time: 153 us
  blocking collectives  86.1 us (56%)
  waiting for transfers between devices  25.8 us (17%)
  Pallas kernels  15.3 us (10%)
  between operations  14.8 us (10%)
  starting transfers between devices  8.74 us (6%)
    all_to_all x3, blocking collectives, exchange(): return lax.all_to_all(blocks, axis, split_axis=0, concat_axis=0, tiled=True)  86.1 us
    all_to_all x2, waiting for transfers between devices, exchange(): return lax.all_to_all(blocks, axis, split_axis=0, concat_axis=0, tiled=True)  25.7 us
    all_to_all x2, starting transfers between devices, exchange(): return lax.all_to_all(blocks, axis, split_axis=0, concat_axis=0, tiled=True)  8.7 us
    pallas_call x1, Pallas kernels, attend(): pl.pallas_call(attend_kernel, out_shape=pltpu.VMEM((16, 256, 128), jnp.bf...  5.79 us
    pallas_call x1, Pallas kernels, ffn(): pl.pallas_call(ffn_kernel, out_shape=pltpu.VMEM((16, 384, 128), jnp.bfloa...  3.77 us
  transfers between devices with their start and end apart: 3, of which 2 were waited for; matrix products, arithmetic and copies ran while one was open for 0% of the time, Pallas kernels for 9%

commit v1 on v0

--- a/solution.py
+++ b/solution.py
@@ -46,51 +46,6 @@
 
 def dot_f32(a, b, dims):
     return lax.dot_general(a, b, (dims, ((), ())), preferred_element_type=jnp.float32)
-
-
-def turn_kernel(q_hbm, k_hbm, v_hbm, cos_ref, sin_ref, q_out, kv_out, q_ref, k_ref, semaphores):
-    copies = start_copies(
-        (q_hbm, k_hbm, v_hbm), (q_ref, k_ref, kv_out.at[:, pl.ds(256, 256)]), semaphores
-    )
-    cos_table = cos_ref[...]
-    sin_table = sin_ref[...]
-
-    def turned(x):
-        x = x.astype(jnp.float32)
-        return (x * cos_table + pltpu.roll(x, 64, 1) * sin_table).astype(jnp.bfloat16)
-
-    for ref, out, copy in ((q_ref, q_out, copies[0]), (k_ref, kv_out, copies[1])):
-        copy.wait()
-        for m in range(2):
-            at = slice(128 * m, 128 * (m + 1))
-            out[:, at] = turned(ref[:, at])
-    copies[2].wait()
-
-
-def turn(q, k, v, offset):
-    rows = q.shape[0]
-    lane = jnp.arange(128, dtype=jnp.int32)
-    inverse = rope_base ** (-2.0 * (lane % 64).astype(jnp.float32) / 128)
-    positions = (offset + jnp.arange(rows, dtype=jnp.int32)).astype(jnp.float32)
-    angles = positions[:, None] * inverse[None, :]
-    cos_table = jnp.cos(angles)
-    sin_table = jnp.sin(angles) * jnp.where(lane < 64, -1.0, 1.0)[None, :]
-    return pl.pallas_call(
-        turn_kernel,
-        out_shape=(
-            pltpu.VMEM((rows, 256), jnp.bfloat16),
-            pltpu.VMEM((rows, 512), jnp.bfloat16),
-        ),
-        compiler_params=pltpu.CompilerParams(vmem_limit_bytes=24 * 2**20),
-        in_specs=hbm(3) + vmem(2),
-        out_specs=tuple(vmem(2)),
-        scratch_shapes=[
-            pltpu.VMEM((rows, 256), jnp.bfloat16),
-            pltpu.VMEM((rows, 256), jnp.bfloat16),
-            pltpu.SemaphoreType.DMA((3,)),
-        ],
-        name="turn",
-    )(far(q), far(k), far(v), near(cos_table), near(sin_table))
 
 
 chunk = 1024
@@ -205,38 +160,79 @@
     return jnp.where(where == index, 1.0, 0.0).reshape(512, 128).astype(jnp.bfloat16)
 
 
-def pack_kernel(tp_ref, *refs):
-    sources, (out_ref, rows_ref, gain_ref, routes_ref, semaphores) = refs[:3], refs[3:]
-    copies = start_copies(sources, (rows_ref, gain_ref, routes_ref), semaphores)
+def begin_kernel(tp_ref, cos_ref, sin_ref, *refs):
+    sources, (q_out, kv_out, packed_out), refs = refs[:6], refs[6:9], refs[9:]
+    q_ref, k_ref, kv_ref, rows_ref, gain_ref, routes_ref, turned_ref = refs[:7]
+    semaphores, out_semaphores = refs[7:]
+    targets = (q_ref, k_ref, kv_ref.at[:, pl.ds(256, 256)], rows_ref, gain_ref, routes_ref)
+    copies = start_copies(sources, targets, semaphores)
+    cos_table = cos_ref[...]
+    sin_table = sin_ref[...]
+
+    def turned(x):
+        x = x.astype(jnp.float32)
+        return (x * cos_table + pltpu.roll(x, 64, 1) * sin_table).astype(jnp.bfloat16)
+
+    for ref, out, copy in ((k_ref, kv_ref, copies[1]), (q_ref, turned_ref, copies[0])):
+        copy.wait()
+        for m in range(2):
+            at = slice(128 * m, 128 * (m + 1))
+            out[:, at] = turned(ref[:, at])
     copies[2].wait()
+    leaving = start_copies((kv_ref, turned_ref), (kv_out, q_out), out_semaphores)
+
+    copies[5].wait()
     first, second, slot = slots_of(routes_ref)
     pick = chosen(first | second, slot)
-    copies[0].wait()
-    copies[1].wait()
+    copies[3].wait()
+    copies[4].wait()
     x = rows_ref[...].astype(jnp.float32)
     inverse = lax.rsqrt(jnp.mean(x * x, axis=1, keepdims=True) + norm_eps)
     start = pl.multiple_of(tp_ref[0] * 128, 128)
     mine = rows_ref[:, pl.ds(start, 128)].astype(jnp.float32)
     normed = (mine * inverse * gain_ref[:, pl.ds(start, 128)]).astype(jnp.bfloat16)
     packed = dot_f32(pick, normed, ((1,), (0,)))
-    out_ref[...] = packed.astype(jnp.bfloat16).reshape(32, 16, 128)
-
-
-def pack(tp, rows, gain, routes_t):
-    return pl.pallas_call(
-        pack_kernel,
-        out_shape=pltpu.VMEM((32, 16, 128), jnp.bfloat16),
+    packed_out[...] = packed.astype(jnp.bfloat16).reshape(32, 16, 128)
+    for copy in leaving:
+        copy.wait()
+
+
+def begin(tp, offset, q, k, v, rows, gain, routes_t):
+    count = q.shape[0]
+    lane = jnp.arange(128, dtype=jnp.int32)
+    inverse = rope_base ** (-2.0 * (lane % 64).astype(jnp.float32) / 128)
+    positions = (offset + jnp.arange(count, dtype=jnp.int32)).astype(jnp.float32)
+    angles = positions[:, None] * inverse[None, :]
+    cos_table = jnp.cos(angles)
+    sin_table = jnp.sin(angles) * jnp.where(lane < 64, -1.0, 1.0)[None, :]
+    return pl.pallas_call(
+        begin_kernel,
+        out_shape=(
+            pltpu.HBM((count, 256), jnp.bfloat16),
+            pltpu.HBM((count, 512), jnp.bfloat16),
+            pltpu.VMEM((32, 16, 128), jnp.bfloat16),
+        ),
         compiler_params=pltpu.CompilerParams(vmem_limit_bytes=24 * 2**20),
-        in_specs=smem(1) + hbm(3),
-        out_specs=vmem(1)[0],
+        in_specs=smem(1) + vmem(2) + hbm(6),
+        out_specs=(*hbm(2), *vmem(1)),
         scratch_shapes=[
+            pltpu.VMEM((count, 256), jnp.bfloat16),
+            pltpu.VMEM((count, 256), jnp.bfloat16),
+            pltpu.VMEM((count, 512), jnp.bfloat16),
             pltpu.VMEM(rows.shape, jnp.bfloat16),
             pltpu.VMEM((1, rows.shape[1]), jnp.float32),
             pltpu.VMEM(routes_t.shape, jnp.int32),
-            pltpu.SemaphoreType.DMA((3,)),
+            pltpu.VMEM((count, 256), jnp.bfloat16),
+            pltpu.SemaphoreType.DMA((6,)),
+            pltpu.SemaphoreType.DMA((2,)),
         ],
-        name="pack",
-    )(tp, far(rows), far(gain.reshape(1, -1)), far(routes_t))
+        name="begin",
+    )(
+        tp,
+        near(cos_table),
+        near(sin_table),
+        *map(far, (q, k, v, rows, gain.reshape(1, -1), routes_t)),
+    )
 
 
 def dense_slots(shape, slot_dim):
@@ -265,19 +261,18 @@
 
 
 def ffn_kernel(rows_ref, *refs):
-    sources, (out_ref, gate_ref, up_ref, down_ref, semaphores) = refs[:3], refs[3:]
-    copies = start_copies(sources, (gate_ref, up_ref, down_ref), semaphores)
+    gate_ref, sources, (out_ref, up_ref, down_ref, semaphores) = refs[0], refs[1:3], refs[3:]
+    copies = start_copies(sources, (up_ref, down_ref), semaphores)
     gate = jnp.zeros((384, 256), jnp.float32)
     up = jnp.zeros((384, 256), jnp.float32)
+    for j in range(8):
+        x = jnp.concatenate([rows_ref[2 * j], rows_ref[2 * j + 1]], axis=1)
+        gate = gate + dot_f32(x, gate_ref[256 * j : 256 * (j + 1), :], ((1,), (0,)))
     copies[0].wait()
     for j in range(8):
         x = jnp.concatenate([rows_ref[2 * j], rows_ref[2 * j + 1]], axis=1)
-        gate = gate + dot_f32(x, gate_ref[256 * j : 256 * (j + 1), :], ((1,), (0,)))
+        up = up + dot_f32(x, up_ref[256 * j : 256 * (j + 1), :], ((1,), (0,)))
     copies[1].wait()
-    for j in range(8):
-        x = jnp.concatenate([rows_ref[2 * j], rows_ref[2 * j + 1]], axis=1)
-        up = up + dot_f32(x, up_ref[256 * j : 256 * (j + 1), :], ((1,), (0,)))
-    copies[2].wait()
     hidden = (gate / (1.0 + jnp.exp(-gate)) * up).astype(jnp.bfloat16)
     for j in range(8):
         part = dot_f32(hidden, down_ref[:, 256 * j : 256 * (j + 1)], ((1,), (0,)))
@@ -291,19 +286,18 @@
         ffn_kernel,
         out_shape=pltpu.VMEM((16, 384, 128), jnp.bfloat16),
         compiler_params=pltpu.CompilerParams(vmem_limit_bytes=24 * 2**20),
-        in_specs=vmem(1) + hbm(3),
+        in_specs=vmem(2) + hbm(2),
         out_specs=vmem(1)[0],
         scratch_shapes=[
-            pltpu.VMEM(gate.shape, jnp.bfloat16),
             pltpu.VMEM(up.shape, jnp.bfloat16),
             pltpu.VMEM(down.shape, jnp.bfloat16),
-            pltpu.SemaphoreType.DMA((3,)),
+            pltpu.SemaphoreType.DMA((2,)),
         ],
         cost_estimate=pl.CostEstimate(
             flops=2 * 384 * 2048 * 768, transcendentals=384 * 256, bytes_accessed=6 * 2**20
         ),
         name="ffn",
-    )(near(rows), far(gate), far(up), far(down))
+    )(near(rows), near(gate), far(up), far(down))
 
 
 def total_kernel(parts_ref, out_ref):
@@ -326,24 +320,45 @@
     )(near(parts))
 
 
-def combine_kernel(returned_ref, routes_ref, weights_ref, out_ref):
+def finish_kernel(parts_ref, returned_ref, routes_hbm, weights_hbm, mixed_out, expert_out, *refs):
+    routes_ref, weights_ref, semaphores = refs
+    copies = start_copies((routes_hbm, weights_hbm), (routes_ref, weights_ref), semaphores)
+    total = parts_ref[0].astype(jnp.float32)
+    for j in range(1, 16):
+        total = total + parts_ref[j].astype(jnp.float32)
+    mixed_out[...] = total.astype(jnp.bfloat16)
+    for copy in copies:
+        copy.wait()
     slots = returned_ref[...].reshape(512, 128)
     first, second, slot = slots_of(routes_ref)
-    one = dot_f32(chosen(first, slot), slots, ((0,), (0,)))
-    two = dot_f32(chosen(second, slot), slots, ((0,), (0,)))
-    out = weights_ref[:, 0:1] * one + weights_ref[:, 1:2] * two
-    out_ref[...] = out.astype(jnp.bfloat16)
-
-
-def combine(returned, routes_t, weights):
-    return pl.pallas_call(
-        combine_kernel,
-        out_shape=jax.ShapeDtypeStruct((128, 128), jnp.bfloat16),
+    row = lax.broadcasted_iota(jnp.int32, (128, 128), 0)
+    col = lax.broadcasted_iota(jnp.int32, (128, 128), 1)
+
+    def picked(k, named):
+        rows = dot_f32(chosen(named, slot), slots, ((0,), (0,)))
+        weights = jnp.where(row == col, weights_ref[k : k + 1, :], 0.0)
+        return jnp.sum(weights, axis=1, keepdims=True) * rows
+
+    expert_out[...] = (picked(0, first) + picked(1, second)).astype(jnp.bfloat16)
+
+
+def finish(parts, returned, routes_t, weights_t):
+    return pl.pallas_call(
+        finish_kernel,
+        out_shape=(
+            jax.ShapeDtypeStruct((256, 128), jnp.bfloat16),
+            jax.ShapeDtypeStruct((128, 128), jnp.bfloat16),
+        ),
         compiler_params=pltpu.CompilerParams(vmem_limit_bytes=24 * 2**20),
-        in_specs=vmem(3),
-        out_specs=vmem(1)[0],
-        name="combine",
-    )(near(returned), routes_t, weights)
+        in_specs=vmem(2) + hbm(2),
+        out_specs=tuple(vmem(2)),
+        scratch_shapes=[
+            pltpu.VMEM(routes_t.shape, jnp.int32),
+            pltpu.VMEM(weights_t.shape, jnp.float32),
+            pltpu.SemaphoreType.DMA((2,)),
+        ],
+        name="finish",
+    )(near(parts), near(returned), far(routes_t), far(weights_t))
 
 
 def exchange(blocks, axis):
@@ -400,9 +415,17 @@
     ep = lax.axis_index("ep")
     tp = lax.axis_index("tp")
     routes_t = routes.T
-    packed = pack(tp.reshape(1), expert_rows, expert_gain, routes_t)
+    own_q, own_kv, packed = begin(
+        tp.reshape(1),
+        ep * query_maps.shape[0],
+        query_maps,
+        key_maps,
+        value_rows,
+        expert_rows,
+        expert_gain,
+        routes_t,
+    )
     arrived = exchange(packed, "ep")
-    own_q, own_kv = turn(query_maps, key_maps, value_rows, ep * query_maps.shape[0])
     kv = lax.all_gather(own_kv, "ep", axis=0, tiled=True)
     gathered = exchange(squeeze(arrived), "tp")
     parts = ffn(gathered, gate_weight, up_weight, down_weight)
@@ -411,9 +434,7 @@
 
     partial_value = attend(ep.reshape(1), head_lambda, own_q, kv, head_gain, out_weight)
     mixed_parts = exchange(partial_value, "tp")
-    mixed = mixed_parts.astype(jnp.float32).sum(axis=0).astype(jnp.bfloat16)
-    expert_out = combine(returned, routes_t, route_weights)
-    return (mixed, expert_out)
+    return finish(mixed_parts, returned, routes_t, route_weights.T)
 
 
 def solution(mesh):

time: 153 us -> 150 us (0.980)
  the two profiles are of different devices: /device:TPU:64 before, /device:TPU:2 now
where the time goes in v1:
time: 150 us; the launch traced here: 149 us
  blocking collectives  104 us (69%)
  between operations  14.8 us (10%)
  waiting for transfers between devices  13.2 us (9%)
  Pallas kernels  11.3 us (8%)
  starting transfers between devices  5.83 us (4%)
    all_to_all x4, blocking collectives, exchange(): return lax.all_to_all(blocks, axis, split_axis=0, concat_axis=0, tiled=True)  104 us
    all_to_all x1, waiting for transfers between devices, exchange(): return lax.all_to_all(blocks, axis, split_axis=0, concat_axis=0, tiled=True)  13.2 us
    all_to_all x1, starting transfers between devices, exchange(): return lax.all_to_all(blocks, axis, split_axis=0, concat_axis=0, tiled=True)  5.79 us
    pallas_call x1, Pallas kernels, attend(): pl.pallas_call(attend_kernel, out_shape=pltpu.VMEM((16, 256, 128), jnp.bf...  3.35 us
  transfers between devices with their start and end apart: 2, of which 1 were waited for; matrix products, arithmetic and copies ran while one was open for 0% of the time, Pallas kernels for 5%

profile of v1, /device:TPU:2, one launch (start us, length us, event | category | flops | bytes accessed | tf_op | source)
XLA Modules:
  0.0 149.3 jit_solution(3252749269821310337)
XLA Ops:
  7.2 0.0 all-gather.2.cloned.1.call-start
  7.2 0.5 fusion
  7.8 2.0 %begin.1 = (bf16[256,256]{1,0:T(8,128)(2,1)}, bf16[256,512]{1,0:T(8,128)(2,1)}, bf16[32,16,128]{2,1,0:T(8,128)(2,1)S(1)}) custom-call(s32[1]{0:T(128)} %bitcast.1.tp_ref, f32[256,128]{1,0:T(8,128)S(1)} %get-tuple-element.9.cos_ref, f32[256,128]{1,0:T(8,128)S(1)} %get-tuple-element.8.sin_ref, bf16[256,256]{1,0:T(8,128)(2,1)} %refs_0_.1, ...), custom_call_target="tpu_custom_call" | custom-call | tf_op jit(solution)/shard_map/begin/pallas_call | solution.py:208
  9.8 0.0 all-gather.2.cloned.1.call-update
  9.9 32.5 %all_to_all.25.arrived_ref = bf16[32,16,128]{2,1,0:T(8,128)(2,1)S(1)} all-to-all(bf16[32,16,128]{2,1,0:T(8,128)(2,1)S(1)} %get-tuple-element.7), channel_id=1, replica_groups=mesh['ep'=32,'tp'=16] {'ep'}, dimensions={0} | all-to-all | bytes 262144 | tf_op jit(solution)/shard_map/all_to_all | solution.py:365
  42.3 0.3 squeeze.13
  42.6 0.0 copy-start
  42.6 28.1 %all_to_all.26.rows_ref = bf16[16,384,128]{2,1,0:T(8,128)(2,1)S(1)} all-to-all(bf16[16,384,128]{2,1,0:T(8,128)(2,1)S(1)} %squeeze.13), channel_id=1, replica_groups=mesh['ep'=32,'tp'=16] {'tp'}, dimensions={0} | all-to-all | bytes 3145728 | tf_op jit(solution)/shard_map/all_to_all | solution.py:365
  70.7 0.0 copy-done
  70.7 2.8 %ffn.1 = bf16[16,384,128]{2,1,0:T(8,128)(2,1)S(1)} custom-call(bf16[16,384,128]{2,1,0:T(8,128)(2,1)S(1)} %all_to_all.26.rows_ref, bf16[2048,256]{1,0:T(8,128)(2,1)S(1)} %bitcast.9, bf16[2048,256]{1,0:T(8,128)(2,1)} %bitcast.10, bf16[256,2048]{1,0:T(8,128)(2,1)} %bitcast.11), custom_call_target="tpu_custom_call" | custom-call | flops 1207959552 | bytes 6291456 | tf_op jit(solution)/shard_map/ffn/pallas_call | solution.py:285
  73.5 23.9 %all_to_all.27.parts_ref = bf16[16,384,128]{2,1,0:T(8,128)(2,1)S(1)} all-to-all(bf16[16,384,128]{2,1,0:T(8,128)(2,1)S(1)} %ffn.1), channel_id=1, replica_groups=mesh['ep'=32,'tp'=16] {'tp'}, dimensions={0} | all-to-all | bytes 3145728 | tf_op jit(solution)/shard_map/all_to_all | solution.py:365
  97.4 1.1 total.1
  98.5 5.8 %all-to-all-start.4 = ((bf16[32,16,128]{2,1,0:T(8,128)(2,1)}), bf16[32,16,128]{2,1,0:T(8,128)(2,1)S(1)}, u32[]{:S(2)}, u32[]{:S(2)}) async-start(bf16[32,16,128]{2,1,0:T(8,128)(2,1)} %total.1), calls=%async_computation.4 | async-start | bytes 262144 | tf_op jit(solution)/shard_map/all_to_all | solution.py:365
  104.9 0.0 all-gather.2.cloned.1.call-done.refs_3_
  105.0 3.3 %attend.1 = bf16[16,256,128]{2,1,0:T(8,128)(2,1)S(1)} custom-call(s32[1]{0:T(128)} %bitcast.ep_ref, f32[1]{0:T(128)S(6)} %copy.15.lam_ref, bf16[256,256]{1,0:T(8,128)(2,1)} %get-tuple-element.5.refs_0_, bf16[256,2048]{1,0:T(8,128)(2,1)} %refs_1_.3, f32[1,256]{1,0:T(1,128)} %bitcast.16, bf16[8192,512]{1,0:T(8,128)(2,1)} %all-gather.2.cloned.1.call-done.refs_3_), custom_call_target="tpu_custom_call" | custom-call | flops 4294967296 | bytes 8388608 | tf_op jit(solution)/shard_map/attend/pallas_call | solution.py:119
  108.3 13.2 %all-to-all-done.4.returned_ref = bf16[32,16,128]{2,1,0:T(8,128)(2,1)S(1)} async-done(((bf16[32,16,128]{2,1,0:T(8,128)(2,1)}), bf16[32,16,128]{2,1,0:T(8,128)(2,1)S(1)}, u32[]{:S(2)}, u32[]{:S(2)}) %all-to-all-start.4) | async-done | bytes 131104 | tf_op jit(solution)/shard_map/all_to_all | solution.py:365
  121.5 19.2 %all_to_all.28.parts_ref = bf16[16,256,128]{2,1,0:T(8,128)(2,1)S(1)} all-to-all(bf16[16,256,128]{2,1,0:T(8,128)(2,1)S(1)} %attend.1), channel_id=1, replica_groups=mesh['ep'=32,'tp'=16] {'tp'}, dimensions={0} | all-to-all | bytes 2097152 | tf_op jit(solution)/shard_map/all_to_all | solution.py:365
  140.7 1.7 %finish.1 = (bf16[256,128]{1,0:T(8,128)(2,1)}, bf16[128,128]{1,0:T(8,128)(2,1)}) custom-call(bf16[16,256,128]{2,1,0:T(8,128)(2,1)S(1)} %all_to_all.28.parts_ref, bf16[32,16,128]{2,1,0:T(8,128)(2,1)S(1)} %all-to-all-done.4.returned_ref, s32[2,128]{1,0:T(2,128)} %bitcast.14, f32[2,128]{1,0:T(2,128)} %bitcast.15), custom_call_target="tpu_custom_call" | custom-call | tf_op jit(solution)/shard_map/finish/pallas_call | solution.py:346
  (2 shorter events, 0.0 us)
Async XLA Ops:
  7.2 97.8 %all-gather.2.cloned.1.call-start = ((), (), s32[]{:S(2)}) async-start(), calls=%async_computation.5 | async-start | bytes 8650752 | tf_op jit(solution)/shard_map/all_gather | solution.py:429
  42.6 28.1 %copy-start = (bf16[1,2048,256]{2,1,0:T(8,128)(2,1)S(1)}, bf16[1,2048,256]{2,1,0:T(8,128)(2,1)}, u32[]{:S(2)}) copy-start(bf16[1,2048,256]{2,1,0:T(8,128)(2,1)} %param.23) | copy-start | bytes 3145732
  98.5 23.0 %all-to-all-start.4 = ((bf16[32,16,128]{2,1,0:T(8,128)(2,1)}), bf16[32,16,128]{2,1,0:T(8,128)(2,1)S(1)}, u32[]{:S(2)}, u32[]{:S(2)}) async-start(bf16[32,16,128]{2,1,0:T(8,128)(2,1)} %total.1), calls=%async_computation.4 | async-start | bytes 262144 | tf_op jit(solution)/shard_map/all_to_all | solution.py:365
Sparse Core Ops, SparseCore 0:
  10.1 84.0 all-gather.1

commit v2 on v1

--- a/solution.py
+++ b/solution.py
@@ -2,6 +2,7 @@
 
 import jax
 import jax.numpy as jnp
+import numpy as np
 from jax import lax
 from jax.experimental import pallas as pl
 from jax.experimental.pallas import tpu as pltpu
@@ -160,14 +161,23 @@
     return jnp.where(where == index, 1.0, 0.0).reshape(512, 128).astype(jnp.bfloat16)
 
 
-def begin_kernel(tp_ref, cos_ref, sin_ref, *refs):
+def begin_kernel(tp_ref, ep_ref, near_hbm, far_hbm, *refs):
     sources, (q_out, kv_out, packed_out), refs = refs[:6], refs[6:9], refs[9:]
     q_ref, k_ref, kv_ref, rows_ref, gain_ref, routes_ref, turned_ref = refs[:7]
-    semaphores, out_semaphores = refs[7:]
+    near_ref, far_ref, semaphores, out_semaphores, table_semaphores = refs[7:]
+    tables = start_copies(
+        (near_hbm, far_hbm.at[ep_ref[0]]), (near_ref, far_ref), table_semaphores
+    )
     targets = (q_ref, k_ref, kv_ref.at[:, pl.ds(256, 256)], rows_ref, gain_ref, routes_ref)
     copies = start_copies(sources, targets, semaphores)
-    cos_table = cos_ref[...]
-    sin_table = sin_ref[...]
+    for copy in tables:
+        copy.wait()
+    cos_near, sin_near = near_ref[:, :128], near_ref[:, 128:]
+    cos_far, sin_far = far_ref[0:1, :], far_ref[1:2, :]
+    cos_table = cos_near * cos_far - sin_near * sin_far
+    sin_table = sin_near * cos_far + cos_near * sin_far
+    lane = lax.broadcasted_iota(jnp.int32, sin_table.shape, 1)
+    sin_table = jnp.where(lane < 64, -sin_table, sin_table)
 
     def turned(x):
         x = x.astype(jnp.float32)
@@ -197,14 +207,18 @@
         copy.wait()
 
 
-def begin(tp, offset, q, k, v, rows, gain, routes_t):
+def angle_tables(count, blocks):
+    inverse = np.tile(rope_base ** (-2.0 * np.arange(64) / 128), 2)
+    within = np.arange(count)[:, None] * inverse
+    starts = (np.arange(blocks) * count)[:, None] * inverse
+    near_table = np.concatenate([np.cos(within), np.sin(within)], axis=1)
+    far_table = np.stack([np.cos(starts), np.sin(starts)], axis=1)
+    return near_table.astype(np.float32), far_table.astype(np.float32)
+
+
+def begin(tp, ep, blocks, q, k, v, rows, gain, routes_t):
     count = q.shape[0]
-    lane = jnp.arange(128, dtype=jnp.int32)
-    inverse = rope_base ** (-2.0 * (lane % 64).astype(jnp.float32) / 128)
-    positions = (offset + jnp.arange(count, dtype=jnp.int32)).astype(jnp.float32)
-    angles = positions[:, None] * inverse[None, :]
-    cos_table = jnp.cos(angles)
-    sin_table = jnp.sin(angles) * jnp.where(lane < 64, -1.0, 1.0)[None, :]
+    near_table, far_table = angle_tables(count, blocks)
     return pl.pallas_call(
         begin_kernel,
         out_shape=(
@@ -213,7 +227,7 @@
             pltpu.VMEM((32, 16, 128), jnp.bfloat16),
         ),
         compiler_params=pltpu.CompilerParams(vmem_limit_bytes=24 * 2**20),
-        in_specs=smem(1) + vmem(2) + hbm(6),
+        in_specs=smem(2) + hbm(8),
         out_specs=(*hbm(2), *vmem(1)),
         scratch_shapes=[
             pltpu.VMEM((count, 256), jnp.bfloat16),
@@ -223,14 +237,18 @@
             pltpu.VMEM((1, rows.shape[1]), jnp.float32),
             pltpu.VMEM(routes_t.shape, jnp.int32),
             pltpu.VMEM((count, 256), jnp.bfloat16),
+            pltpu.VMEM((count, 256), jnp.float32),
+            pltpu.VMEM((2, 128), jnp.float32),
             pltpu.SemaphoreType.DMA((6,)),
+            pltpu.SemaphoreType.DMA((2,)),
             pltpu.SemaphoreType.DMA((2,)),
         ],
         name="begin",
     )(
         tp,
-        near(cos_table),
-        near(sin_table),
+        ep,
+        far(jnp.asarray(near_table)),
+        far(jnp.asarray(far_table)),
         *map(far, (q, k, v, rows, gain.reshape(1, -1), routes_t)),
     )
 
@@ -417,7 +435,8 @@
     routes_t = routes.T
     own_q, own_kv, packed = begin(
         tp.reshape(1),
-        ep * query_maps.shape[0],
+        ep.reshape(1),
+        lax.axis_size("ep"),
         query_maps,
         key_maps,
         value_rows,

time: 150 us -> 150 us (level)
  no operation moved by 1% of the time
where the time goes in v2:
time: 150 us; the launch traced here: 149 us
  blocking collectives  103 us (69%)
  between operations  14.8 us (10%)
  waiting for transfers between devices  13.2 us (9%)
  Pallas kernels  11.8 us (8%)
  starting transfers between devices  6.12 us (4%)
    all_to_all x4, blocking collectives, exchange(): return lax.all_to_all(blocks, axis, split_axis=0, concat_axis=0, tiled=True)  103 us
    all_to_all x1, waiting for transfers between devices, exchange(): return lax.all_to_all(blocks, axis, split_axis=0, concat_axis=0, tiled=True)  13.2 us
    all_to_all x1, starting transfers between devices, exchange(): return lax.all_to_all(blocks, axis, split_axis=0, concat_axis=0, tiled=True)  6.09 us
    pallas_call x1, Pallas kernels, attend(): pl.pallas_call(attend_kernel, out_shape=pltpu.VMEM((16, 256, 128), jnp.bf...  3.35 us
  transfers between devices with their start and end apart: 2, of which 1 were waited for; matrix products, arithmetic and copies ran while one was open for 0% of the time, Pallas kernels for 5%

profile of v2, /device:TPU:2, one launch (start us, length us, event | category | flops | bytes accessed | tf_op | source)
XLA Modules:
  0.0 149.3 jit_solution(11921551751516269622)
XLA Ops:
  7.2 0.0 all-gather.2.cloned.1.call-start
  7.2 2.5 %begin.1 = (bf16[256,256]{1,0:T(8,128)(2,1)}, bf16[256,512]{1,0:T(8,128)(2,1)}, bf16[32,16,128]{2,1,0:T(8,128)(2,1)S(1)}) custom-call(s32[1]{0:T(128)} %bitcast.1.tp_ref, s32[1]{0:T(128)} %bitcast.ep_ref, f32[256,256]{1,0:T(8,128)} %constant.13.clone.near_hbm, f32[32,2,128]{2,1,0:T(2,128)} %constant.14.clone.far_hbm, bf16[256,256]{1,0:T(8,128)(2,1)} %refs_0_.1, ...), custom_call_target="tpu_custom_call" | custom-call | tf_op jit(solution)/shard_map/begin/pallas_call | solution.py:222
  9.7 0.0 all-gather.2.cloned.1.call-update
  9.7 32.5 %all_to_all.25.arrived_ref = bf16[32,16,128]{2,1,0:T(8,128)(2,1)S(1)} all-to-all(bf16[32,16,128]{2,1,0:T(8,128)(2,1)S(1)} %get-tuple-element.7), channel_id=1, replica_groups=mesh['ep'=32,'tp'=16] {'ep'}, dimensions={0} | all-to-all | bytes 262144 | tf_op jit(solution)/shard_map/all_to_all | solution.py:383
  42.2 0.3 squeeze.13
  42.5 0.0 copy-start
  42.5 28.0 %all_to_all.26.rows_ref = bf16[16,384,128]{2,1,0:T(8,128)(2,1)S(1)} all-to-all(bf16[16,384,128]{2,1,0:T(8,128)(2,1)S(1)} %squeeze.13), channel_id=1, replica_groups=mesh['ep'=32,'tp'=16] {'tp'}, dimensions={0} | all-to-all | bytes 3145728 | tf_op jit(solution)/shard_map/all_to_all | solution.py:383
  70.6 0.0 copy-done
  70.6 2.8 %ffn.1 = bf16[16,384,128]{2,1,0:T(8,128)(2,1)S(1)} custom-call(bf16[16,384,128]{2,1,0:T(8,128)(2,1)S(1)} %all_to_all.26.rows_ref, bf16[2048,256]{1,0:T(8,128)(2,1)S(1)} %bitcast.9, bf16[2048,256]{1,0:T(8,128)(2,1)} %bitcast.10, bf16[256,2048]{1,0:T(8,128)(2,1)} %bitcast.11), custom_call_target="tpu_custom_call" | custom-call | flops 1207959552 | bytes 6291456 | tf_op jit(solution)/shard_map/ffn/pallas_call | solution.py:303
  73.4 23.8 %all_to_all.27.parts_ref = bf16[16,384,128]{2,1,0:T(8,128)(2,1)S(1)} all-to-all(bf16[16,384,128]{2,1,0:T(8,128)(2,1)S(1)} %ffn.1), channel_id=1, replica_groups=mesh['ep'=32,'tp'=16] {'tp'}, dimensions={0} | all-to-all | bytes 3145728 | tf_op jit(solution)/shard_map/all_to_all | solution.py:383
  97.2 1.1 total.1
  98.3 6.1 %all-to-all-start.4 = ((bf16[32,16,128]{2,1,0:T(8,128)(2,1)}), bf16[32,16,128]{2,1,0:T(8,128)(2,1)S(1)}, u32[]{:S(2)}, u32[]{:S(2)}) async-start(bf16[32,16,128]{2,1,0:T(8,128)(2,1)} %total.1), calls=%async_computation.4 | async-start | bytes 262144 | tf_op jit(solution)/shard_map/all_to_all | solution.py:383
  105.0 0.0 all-gather.2.cloned.1.call-done.refs_3_
  105.1 3.3 %attend.1 = bf16[16,256,128]{2,1,0:T(8,128)(2,1)S(1)} custom-call(s32[1]{0:T(128)} %bitcast.ep_ref, f32[1]{0:T(128)S(6)} %copy.17.lam_ref, bf16[256,256]{1,0:T(8,128)(2,1)} %get-tuple-element.5.refs_0_, bf16[256,2048]{1,0:T(8,128)(2,1)} %refs_1_.3, f32[1,256]{1,0:T(1,128)} %bitcast.16, bf16[8192,512]{1,0:T(8,128)(2,1)} %all-gather.2.cloned.1.call-done.refs_3_), custom_call_target="tpu_custom_call" | custom-call | flops 4294967296 | bytes 8388608 | tf_op jit(solution)/shard_map/attend/pallas_call | solution.py:120
  108.4 13.2 %all-to-all-done.4.returned_ref = bf16[32,16,128]{2,1,0:T(8,128)(2,1)S(1)} async-done(((bf16[32,16,128]{2,1,0:T(8,128)(2,1)}), bf16[32,16,128]{2,1,0:T(8,128)(2,1)S(1)}, u32[]{:S(2)}, u32[]{:S(2)}) %all-to-all-start.4) | async-done | bytes 131104 | tf_op jit(solution)/shard_map/all_to_all | solution.py:383
  121.6 19.1 %all_to_all.28.parts_ref = bf16[16,256,128]{2,1,0:T(8,128)(2,1)S(1)} all-to-all(bf16[16,256,128]{2,1,0:T(8,128)(2,1)S(1)} %attend.1), channel_id=1, replica_groups=mesh['ep'=32,'tp'=16] {'tp'}, dimensions={0} | all-to-all | bytes 2097152 | tf_op jit(solution)/shard_map/all_to_all | solution.py:383
  140.7 1.7 %finish.1 = (bf16[256,128]{1,0:T(8,128)(2,1)}, bf16[128,128]{1,0:T(8,128)(2,1)}) custom-call(bf16[16,256,128]{2,1,0:T(8,128)(2,1)S(1)} %all_to_all.28.parts_ref, bf16[32,16,128]{2,1,0:T(8,128)(2,1)S(1)} %all-to-all-done.4.returned_ref, s32[2,128]{1,0:T(2,128)} %bitcast.14, f32[2,128]{1,0:T(2,128)} %bitcast.15), custom_call_target="tpu_custom_call" | custom-call | tf_op jit(solution)/shard_map/finish/pallas_call | solution.py:364
Async XLA Ops:
  7.2 97.9 %all-gather.2.cloned.1.call-start = ((), (), s32[]{:S(2)}) async-start(), calls=%async_computation.5 | async-start | bytes 8650752 | tf_op jit(solution)/shard_map/all_gather | solution.py:448
  42.5 28.0 %copy-start = (bf16[1,2048,256]{2,1,0:T(8,128)(2,1)S(1)}, bf16[1,2048,256]{2,1,0:T(8,128)(2,1)}, u32[]{:S(2)}) copy-start(bf16[1,2048,256]{2,1,0:T(8,128)(2,1)} %param.25) | copy-start | bytes 3145732
  98.3 23.3 %all-to-all-start.4 = ((bf16[32,16,128]{2,1,0:T(8,128)(2,1)}), bf16[32,16,128]{2,1,0:T(8,128)(2,1)S(1)}, u32[]{:S(2)}, u32[]{:S(2)}) async-start(bf16[32,16,128]{2,1,0:T(8,128)(2,1)} %total.1), calls=%async_computation.4 | async-start | bytes 262144 | tf_op jit(solution)/shard_map/all_to_all | solution.py:383
Sparse Core Ops, SparseCore 0:
  10.1 83.5 all-gather.1

commit v3 on v2

--- a/solution.py
+++ b/solution.py
@@ -338,29 +338,48 @@
     )(near(parts))
 
 
-def finish_kernel(parts_ref, returned_ref, routes_hbm, weights_hbm, mixed_out, expert_out, *refs):
-    routes_ref, weights_ref, semaphores = refs
-    copies = start_copies((routes_hbm, weights_hbm), (routes_ref, weights_ref), semaphores)
+def plan_kernel(routes_ref, weights_ref, one_out, two_out, scale_out):
+    first, second, slot = slots_of(routes_ref)
+    index = lax.broadcasted_iota(jnp.int32, (32, 16, 128), 1)
+    for named, out in ((first, one_out), (second, two_out)):
+        where = jnp.where(named, slot, -1)[:, None, :]
+        pick = jnp.where(where == index, 1.0, 0.0).reshape(512, 128)
+        out[...] = pick.T.astype(jnp.bfloat16)
+    row = lax.broadcasted_iota(jnp.int32, (128, 128), 0)
+    col = lax.broadcasted_iota(jnp.int32, (128, 128), 1)
+    for k in range(2):
+        weights = jnp.where(row == col, weights_ref[k : k + 1, :], 0.0)
+        column = jnp.sum(weights, axis=1, keepdims=True)
+        scale_out[:, 128 * k : 128 * (k + 1)] = jnp.broadcast_to(column, (128, 128))
+
+
+def plan(routes_t, weights_t):
+    return pl.pallas_call(
+        plan_kernel,
+        out_shape=(
+            pltpu.VMEM((128, 512), jnp.bfloat16),
+            pltpu.VMEM((128, 512), jnp.bfloat16),
+            pltpu.VMEM((128, 256), jnp.float32),
+        ),
+        compiler_params=pltpu.CompilerParams(vmem_limit_bytes=24 * 2**20),
+        in_specs=vmem(2),
+        out_specs=tuple(vmem(3)),
+        name="plan",
+    )(far(routes_t), far(weights_t))
+
+
+def finish_kernel(parts_ref, returned_ref, one_ref, two_ref, scale_ref, mixed_out, expert_out):
     total = parts_ref[0].astype(jnp.float32)
     for j in range(1, 16):
         total = total + parts_ref[j].astype(jnp.float32)
     mixed_out[...] = total.astype(jnp.bfloat16)
-    for copy in copies:
-        copy.wait()
     slots = returned_ref[...].reshape(512, 128)
-    first, second, slot = slots_of(routes_ref)
-    row = lax.broadcasted_iota(jnp.int32, (128, 128), 0)
-    col = lax.broadcasted_iota(jnp.int32, (128, 128), 1)
-
-    def picked(k, named):
-        rows = dot_f32(chosen(named, slot), slots, ((0,), (0,)))
-        weights = jnp.where(row == col, weights_ref[k : k + 1, :], 0.0)
-        return jnp.sum(weights, axis=1, keepdims=True) * rows
-
-    expert_out[...] = (picked(0, first) + picked(1, second)).astype(jnp.bfloat16)
-
-
-def finish(parts, returned, routes_t, weights_t):
+    one = dot_f32(one_ref[...], slots, ((1,), (0,)))
+    two = dot_f32(two_ref[...], slots, ((1,), (0,)))
+    expert_out[...] = (scale_ref[:, :128] * one + scale_ref[:, 128:] * two).astype(jnp.bfloat16)
+
+
+def finish(parts, returned, planned):
     return pl.pallas_call(
         finish_kernel,
         out_shape=(
@@ -368,15 +387,10 @@
             jax.ShapeDtypeStruct((128, 128), jnp.bfloat16),
         ),
         compiler_params=pltpu.CompilerParams(vmem_limit_bytes=24 * 2**20),
-        in_specs=vmem(2) + hbm(2),
+        in_specs=vmem(5),
         out_specs=tuple(vmem(2)),
-        scratch_shapes=[
-            pltpu.VMEM(routes_t.shape, jnp.int32),
-            pltpu.VMEM(weights_t.shape, jnp.float32),
-            pltpu.SemaphoreType.DMA((2,)),
-        ],
         name="finish",
-    )(near(parts), near(returned), far(routes_t), far(weights_t))
+    )(near(parts), near(returned), *map(near, planned))
 
 
 def exchange(blocks, axis):
@@ -453,7 +467,7 @@
 
     partial_value = attend(ep.reshape(1), head_lambda, own_q, kv, head_gain, out_weight)
     mixed_parts = exchange(partial_value, "tp")
-    return finish(mixed_parts, returned, routes_t, route_weights.T)
+    return finish(mixed_parts, returned, plan(routes_t, route_weights.T))
 
 
 def solution(mesh):

time: 150 us -> 150 us (level)
  the two profiles are of different devices: /device:TPU:2 before, /device:TPU:64 now
where the time goes in v3:
time: 150 us; the launch traced here: 149 us
  blocking collectives  84.4 us (56%)
  waiting for transfers between devices  25.9 us (17%)
  between operations  14.7 us (10%)
  Pallas kernels  14.4 us (10%)
  starting transfers between devices  9.92 us (7%)
    all_to_all x3, blocking collectives, exchange(): return lax.all_to_all(blocks, axis, split_axis=0, concat_axis=0, tiled=True)  84.4 us
    all_to_all x2, waiting for transfers between devices, exchange(): return lax.all_to_all(blocks, axis, split_axis=0, concat_axis=0, tiled=True)  25.9 us
    all_to_all x2, starting transfers between devices, exchange(): return lax.all_to_all(blocks, axis, split_axis=0, concat_axis=0, tiled=True)  9.88 us
    pallas_call x1, Pallas kernels, attend(): pl.pallas_call(attend_kernel, out_shape=pltpu.VMEM((16, 256, 128), jnp.bf...  5.78 us
  transfers between devices with their start and end apart: 3, of which 2 were waited for; matrix products, arithmetic and copies ran while one was open for 0% of the time, Pallas kernels for 7%

profile of v3, /device:TPU:64, one launch (start us, length us, event | category | flops | bytes accessed | tf_op | source)
XLA Modules:
  0.0 149.4 jit_solution(825662776927464865)
XLA Ops:
  7.2 0.0 all-gather.2.cloned.1.call-start
  7.2 2.5 %begin.1 = (bf16[256,256]{1,0:T(8,128)(2,1)}, bf16[256,512]{1,0:T(8,128)(2,1)}, bf16[32,16,128]{2,1,0:T(8,128)(2,1)S(1)}) custom-call(s32[1]{0:T(128)} %bitcast.1.tp_ref, s32[1]{0:T(128)} %bitcast.ep_ref, f32[256,256]{1,0:T(8,128)} %constant.13.clone.near_hbm, f32[32,2,128]{2,1,0:T(2,128)} %constant.14.clone.far_hbm, bf16[256,256]{1,0:T(8,128)(2,1)} %refs_0_.1, ...), custom_call_target="tpu_custom_call" | custom-call | tf_op jit(solution)/shard_map/begin/pallas_call | solution.py:222
  9.7 0.0 all-gather.2.cloned.1.call-update
  9.7 28.9 %all_to_all.25.arrived_ref = bf16[32,16,128]{2,1,0:T(8,128)(2,1)S(1)} all-to-all(bf16[32,16,128]{2,1,0:T(8,128)(2,1)S(1)} %get-tuple-element.10), channel_id=1, replica_groups=mesh['ep'=32,'tp'=16] {'ep'}, dimensions={0} | all-to-all | bytes 262144 | tf_op jit(solution)/shard_map/all_to_all | solution.py:397
  38.6 0.3 squeeze.13
  38.9 0.0 copy-start
  38.9 30.4 %all_to_all.26.rows_ref = bf16[16,384,128]{2,1,0:T(8,128)(2,1)S(1)} all-to-all(bf16[16,384,128]{2,1,0:T(8,128)(2,1)S(1)} %squeeze.13), channel_id=1, replica_groups=mesh['ep'=32,'tp'=16] {'tp'}, dimensions={0} | all-to-all | bytes 3145728 | tf_op jit(solution)/shard_map/all_to_all | solution.py:397
  69.3 0.0 copy-done
  69.3 2.8 %ffn.1 = bf16[16,384,128]{2,1,0:T(8,128)(2,1)S(1)} custom-call(bf16[16,384,128]{2,1,0:T(8,128)(2,1)S(1)} %all_to_all.26.rows_ref, bf16[2048,256]{1,0:T(8,128)(2,1)S(1)} %bitcast.9, bf16[2048,256]{1,0:T(8,128)(2,1)} %bitcast.10, bf16[256,2048]{1,0:T(8,128)(2,1)} %bitcast.11), custom_call_target="tpu_custom_call" | custom-call | flops 1207959552 | bytes 6291456 | tf_op jit(solution)/shard_map/ffn/pallas_call | solution.py:303
  72.1 25.1 %all_to_all.27.parts_ref = bf16[16,384,128]{2,1,0:T(8,128)(2,1)S(1)} all-to-all(bf16[16,384,128]{2,1,0:T(8,128)(2,1)S(1)} %ffn.1), channel_id=1, replica_groups=mesh['ep'=32,'tp'=16] {'tp'}, dimensions={0} | all-to-all | bytes 3145728 | tf_op jit(solution)/shard_map/all_to_all | solution.py:397
  97.3 1.1 total.1
  98.4 6.2 %all-to-all-start.4 = ((bf16[32,16,128]{2,1,0:T(8,128)(2,1)}), bf16[32,16,128]{2,1,0:T(8,128)(2,1)S(1)}, u32[]{:S(2)}, u32[]{:S(2)}) async-start(bf16[32,16,128]{2,1,0:T(8,128)(2,1)} %total.1), calls=%async_computation.4 | async-start | bytes 262144 | tf_op jit(solution)/shard_map/all_to_all | solution.py:397
  105.2 0.0 all-gather.2.cloned.1.call-done.refs_3_
  105.3 5.8 %attend.1 = bf16[16,256,128]{2,1,0:T(8,128)(2,1)} custom-call(s32[1]{0:T(128)} %bitcast.ep_ref, f32[1]{0:T(128)S(6)} %copy.17.lam_ref, bf16[256,256]{1,0:T(8,128)(2,1)} %get-tuple-element.8.refs_0_, bf16[256,2048]{1,0:T(8,128)(2,1)} %refs_1_.3, f32[1,256]{1,0:T(1,128)} %bitcast.16, bf16[8192,512]{1,0:T(8,128)(2,1)} %all-gather.2.cloned.1.call-done.refs_3_), custom_call_target="tpu_custom_call" | custom-call | flops 4294967296 | bytes 8388608 | tf_op jit(solution)/shard_map/attend/pallas_call | solution.py:120
  111.1 7.7 %all-to-all-done.4.returned_ref = bf16[32,16,128]{2,1,0:T(8,128)(2,1)S(1)} async-done(((bf16[32,16,128]{2,1,0:T(8,128)(2,1)}), bf16[32,16,128]{2,1,0:T(8,128)(2,1)S(1)}, u32[]{:S(2)}, u32[]{:S(2)}) %all-to-all-start.4) | async-done | bytes 131104 | tf_op jit(solution)/shard_map/all_to_all | solution.py:397
  118.8 3.7 %all-to-all-start = ((bf16[16,256,128]{2,1,0:T(8,128)(2,1)}), bf16[16,256,128]{2,1,0:T(8,128)(2,1)S(1)}, u32[]{:S(2)}, u32[]{:S(2)}) async-start(bf16[16,256,128]{2,1,0:T(8,128)(2,1)} %attend.1), calls=%async_computation | async-start | bytes 2097152 | tf_op jit(solution)/shard_map/all_to_all | solution.py:397
  122.4 1.0 plan.1
  123.4 18.2 %all-to-all-done.parts_ref = bf16[16,256,128]{2,1,0:T(8,128)(2,1)S(1)} async-done(((bf16[16,256,128]{2,1,0:T(8,128)(2,1)}), bf16[16,256,128]{2,1,0:T(8,128)(2,1)S(1)}, u32[]{:S(2)}, u32[]{:S(2)}) %all-to-all-start) | async-done | bytes 1048608 | tf_op jit(solution)/shard_map/all_to_all | solution.py:397
  141.6 0.9 finish.1
Async XLA Ops:
  7.2 98.1 %all-gather.2.cloned.1.call-start = ((), (), s32[]{:S(2)}) async-start(), calls=%async_computation.5 | async-start | bytes 8650752 | tf_op jit(solution)/shard_map/all_gather | solution.py:462
  38.9 30.4 %copy-start = (bf16[1,2048,256]{2,1,0:T(8,128)(2,1)S(1)}, bf16[1,2048,256]{2,1,0:T(8,128)(2,1)}, u32[]{:S(2)}) copy-start(bf16[1,2048,256]{2,1,0:T(8,128)(2,1)} %param.25) | copy-start | bytes 3145732
  98.4 20.4 %all-to-all-start.4 = ((bf16[32,16,128]{2,1,0:T(8,128)(2,1)}), bf16[32,16,128]{2,1,0:T(8,128)(2,1)S(1)}, u32[]{:S(2)}, u32[]{:S(2)}) async-start(bf16[32,16,128]{2,1,0:T(8,128)(2,1)} %total.1), calls=%async_computation.4 | async-start | bytes 262144 | tf_op jit(solution)/shard_map/all_to_all | solution.py:397
  118.8 22.9 %all-to-all-start = ((bf16[16,256,128]{2,1,0:T(8,128)(2,1)}), bf16[16,256,128]{2,1,0:T(8,128)(2,1)S(1)}, u32[]{:S(2)}, u32[]{:S(2)}) async-start(bf16[16,256,128]{2,1,0:T(8,128)(2,1)} %attend.1), calls=%async_computation | async-start | bytes 2097152 | tf_op jit(solution)/shard_map/all_to_all | solution.py:397
Sparse Core Ops, SparseCore 0:
  10.1 82.0 all-gather.1
